TPU v7x, 32 devices: a whole 2x2x4 slice. The times are simulated.
32 devices in a mesh: row: 4 (over z), col: 8 (over y, x, core).
Axes of the slice: x: 2, y: 2, z: 4, core: 2. Of those that a mesh axis runs over, the one named last changes fastest.
Arguments:
- tokens: bfloat16 [32, 144, 2048], P('row', 'col'), may hold values from -6 to 6
- norm_gain: bfloat16 [2048], replicated, may hold values from 0.099609375 to 1.8984375
- w_in: bfloat16 [2048, 1152], replicated, may hold values from -0.125 to 0.125
- w_out: bfloat16 [1152, 2048], replicated, may hold values from -0.1875 to 0.1875
Outputs:
- mixed: bfloat16 [144, 32, 2048], P('row', 'col')
All inputs are finite; a program needn't handle non-finite values.
Results may differ from a plain program's by a relative error of at most 0.013.
Values may be sent and summed in bfloat16 or wider, within the bound.
A program may use at most 64 MiB of HBM per device.

v0:
```python
import math

import jax
import jax.numpy as jnp
from jax import lax
from jax.sharding import PartitionSpec as P

GROUP = 128


norm_eps = 1e-06
highest = lax.Precision.HIGHEST


def tables(length):
    series = jnp.arange(length, dtype=jnp.int32)
    product = series[:, None] * series[None, :] % length
    angles = product.astype(jnp.float32) * (2.0 * math.pi / length)
    return (jnp.cos(angles), jnp.sin(angles))


def folded_order(length_first, devices):
    block = length_first // devices
    half_block = block // 2
    series = jnp.arange(length_first, dtype=jnp.int32)
    device = series // block
    inner = series % block
    lower = device * half_block + inner
    upper = length_first - device * half_block - (inner - half_block)
    upper = jnp.where((device == 0) & (inner == half_block), length_first // 2, upper)
    return jnp.where(inner < half_block, lower, upper) % length_first


def to_channels(values, row_count):
    rows_first, rows_second, channels = values.shape
    width = channels // row_count
    parted = values.reshape(rows_first, rows_second, row_count, width).transpose(2, 0, 1, 3)
    return parted.reshape(row_count * rows_first, rows_second * width)


def product(table, values):
    return jnp.dot(table, values, precision=highest)


def middle(real_part, imag_part, width):
    length_first = real_part.shape[0]
    rows_second = real_part.shape[1] // width
    col_count = lax.axis_size("col")
    length_second = rows_second * col_count
    positions = length_first * length_second
    frequency = folded_order(length_first, col_count)
    series = jnp.arange(length_first, dtype=jnp.int32)
    first_angle = (frequency[:, None] * series[None, :] % length_first).astype(jnp.float32)
    first_angle = first_angle * (2.0 * math.pi / length_first)
    first_cos = jnp.cos(first_angle)
    first_sin = jnp.sin(first_angle)
    first_real = product(first_cos, real_part)
    first_imag = -product(first_sin, real_part)
    first_real = first_real + product(first_sin, imag_part)
    first_imag = first_imag + product(first_cos, imag_part)
    first_real = first_real.reshape(length_first, rows_second, width)
    first_imag = first_imag.reshape(length_first, rows_second, width)
    second_index = lax.axis_index("col") * rows_second + jnp.arange(rows_second, dtype=jnp.int32)
    twiddle_angle = (frequency[:, None] * second_index[None, :] % positions).astype(jnp.float32)
    twiddle_angle = twiddle_angle * (2.0 * math.pi / positions)
    twiddle_cos = jnp.cos(twiddle_angle)[:, :, None]
    twiddle_sin = jnp.sin(twiddle_angle)[:, :, None]
    turned_real = first_real * twiddle_cos + first_imag * twiddle_sin
    turned_imag = first_imag * twiddle_cos - first_real * twiddle_sin
    turned = jnp.stack([turned_real, turned_imag]).transpose(0, 2, 1, 3)
    turned = turned.reshape(2, rows_second, length_first * width)
    exchanged = lax.all_to_all(
        turned.astype(jnp.bfloat16), "col", split_axis=2, concat_axis=1, tiled=True
    ).astype(turned.dtype)
    second_cos, second_sin = tables(length_second)
    block = length_first // col_count
    out_shape = (length_second, block, width)
    out_real = (product(second_cos, exchanged[0]) + product(second_sin, exchanged[1])).reshape(
        out_shape
    )
    return out_real


def shards(tokens, norm_gain, w_in, w_out):
    rows_first, rows_second, features = tokens.shape
    row_count = lax.axis_size("row")
    length_first = rows_first * row_count
    length_second = rows_second * lax.axis_size("col")
    channels = w_in.shape[1]
    width = channels // row_count
    groups = channels // GROUP
    scaling = 1.0 / math.sqrt(length_first * length_second * GROUP)
    floats = tokens.astype(jnp.float32)
    normed = (
        floats
        * lax.rsqrt(jnp.mean(floats * floats, axis=-1, keepdims=True) + norm_eps)
        * norm_gain.astype(jnp.float32)
    ).astype(jnp.bfloat16)
    mapped = jnp.dot(normed.reshape(-1, features), w_in, preferred_element_type=jnp.float32)
    mapped = mapped.astype(jnp.bfloat16).reshape(rows_first, rows_second, channels)
    channel_cos, channel_sin = tables(GROUP)
    grouped = mapped.astype(jnp.float32).reshape(rows_first, rows_second, groups, GROUP)
    spec_real = jnp.einsum("abgj,jm->abgm", grouped, channel_cos, precision=highest)
    spec_imag = -jnp.einsum("abgj,jm->abgm", grouped, channel_sin, precision=highest)
    stacked = jnp.stack(
        [
            to_channels(spec_real.reshape(rows_first, rows_second, channels), row_count),
            to_channels(spec_imag.reshape(rows_first, rows_second, channels), row_count),
        ]
    )
    arrived = lax.all_to_all(
        stacked.astype(jnp.bfloat16), "row", split_axis=1, concat_axis=1, tiled=True
    ).astype(stacked.dtype)
    result = middle(arrived[0], arrived[1], width)
    spectrum = (result * scaling).astype(jnp.bfloat16)
    returned = lax.all_to_all(spectrum, "row", split_axis=0, concat_axis=2, tiled=True)
    mixed = jnp.dot(returned.reshape(-1, channels), w_out, preferred_element_type=jnp.float32)
    return mixed.astype(jnp.bfloat16).reshape(returned.shape[0], returned.shape[1], features)


def solution(mesh):
    in_specs = (P("row", "col", None), P(), P(), P())
    out_specs = P("row", "col", None)
    return jax.shard_map(shards, mesh=mesh, in_specs=in_specs, out_specs=out_specs, check_vma=False)
```

profile of v0, /device:TPU:0, one launch (start us, length us, event | category | flops | bytes accessed | tf_op | source)
XLA Modules:
  0.0 115.7 jit_solution(10309943882947872754)
XLA Ops:
  0.0 0.7 convert_element_type.64
  0.7 1.3 %fusion.3 = f32[8,18]{0,1:T(8,128)S(1)} fusion(bf16[8,18,2048]{2,0,1:T(8,128)(2,1)} %param.4), kind=kLoop, calls=%fused_computation.13 | loop fusion | flops 884592 | bytes 590400 | tf_op jit(solution)/shard_map/reduce_sum | solution.py:96
  2.0 1.3 %fusion.5 = bf16[8,18,2048]{2,0,1:T(8,128)(2,1)S(1)} fusion(bf16[8,18,2048]{2,0,1:T(8,128)(2,1)} %param.4, f32[2048]{0:T(1024)S(1)} %convert_element_type.64, f32[8,18]{0,1:T(8,128)S(1)} %add_rsqrt_fusion), kind=kLoop, calls=%fused_computation.15 | loop fusion | flops 1179648 | bytes 1188416 | tf_op jit(solution)/shard_map/convert_element_type | solution.py:98
  3.2 0.3 copy.58
  3.8 3.3 %convolution_convert_fusion.1 = bf16[144,1152]{1,0:T(8,128)(2,1)S(1)} fusion(bf16[144,2048]{1,0:T(8,128)(2,1)S(1)} %reshape.195, bf16[2048,1152]{1,0:T(8,128)(2,1)} %param.6), kind=kOutput, calls=%fused_computation.7 | convolution fusion | flops 679643136 | bytes 5640192 | tf_op jit(solution)/shard_map/dot_general | solution.py:99
  7.3 0.8 fusion.2
  8.0 0.8 convolution_convert_fusion.2
  8.9 0.7 reshape_reshape.8
  10.1 0.7 reshape_reshape.9
  10.9 0.3 stack_reshape.9
  11.3 1.4 %copy.65 = bf16[2,32,5184]{2,0,1:T(2,128)(2,1)} copy(bf16[2,32,5184]{2,1,0:T(8,128)(2,1)S(1)} %pad_maximum_fusion) | data formatting | bytes 1327104 | tf_op jit(solution)/shard_map/stack | solution.py:105
  12.7 6.3 %all-to-all-start = ((bf16[2,32,5184]{2,0,1:T(2,128)(2,1)}), bf16[2,32,5184]{2,0,1:T(2,128)(2,1)S(1)}, u32[]{:S(2)}, u32[]{:S(2)}) async-start(bf16[2,32,5184]{2,0,1:T(2,128)(2,1)} %copy.65), calls=%async_computation | async-start | bytes 1343488 | tf_op jit(solution)/shard_map/all_to_all | solution.py:111
  19.2 17.5 %all-to-all-done = bf16[2,32,5184]{2,0,1:T(2,128)(2,1)S(1)} async-done(((bf16[2,32,5184]{2,0,1:T(2,128)(2,1)}), bf16[2,32,5184]{2,0,1:T(2,128)(2,1)S(1)}, u32[]{:S(2)}, u32[]{:S(2)}) %all-to-all-start) | async-done | bytes 663584 | tf_op jit(solution)/shard_map/all_to_all | solution.py:111
  36.7 0.9 fusion.87
  37.6 0.6 convolution_negate_fusion
  38.2 0.6 fusion.18
  38.8 0.6 convolution_add_fusion.1
  39.4 0.6 convolution_add_fusion
  40.0 0.6 reshape.198
  40.6 0.6 reshape.197
  41.1 0.4 add_convert_fusion
  41.8 7.9 %copy.76 = bf16[2,18,32,288]{1,0,3,2:T(2,128)(2,1)} copy(bf16[2,18,32,288]{3,1,2,0:T(8,128)(2,1)S(1)} %maximum_bitcast_fusion) | data formatting | bytes 1327104 | tf_op jit(solution)/shard_map/convert_element_type | solution.py:73
  49.7 8.7 %reshape.203 = bf16[8,2,20736]{2,1,0:T(2,128)(2,1)S(1)} reshape(bf16[9216,2,18]{2,1,0:T(2,128)(2,1)} %bitcast.36) | data formatting | bytes 1327104
  58.4 14.7 %all_to_all.35 = bf16[8,2,20736]{2,1,0:T(2,128)(2,1)S(1)} all-to-all(bf16[8,2,20736]{2,1,0:T(2,128)(2,1)S(1)} %reshape.203), channel_id=1, replica_groups=mesh['row'=4,'col'=8] {'col'}, dimensions={0} | all-to-all | bytes 1327104 | tf_op jit(solution)/shard_map/all_to_all | solution.py:72
  73.2 12.6 %reshape.204 = bf16[9216,2,18]{2,1,0:T(2,128)(2,1)} reshape(bf16[8,2,20736]{2,1,0:T(2,128)(2,1)S(1)} %all_to_all.35) | data formatting | bytes 1327104
  85.8 7.1 %copy.77 = bf16[2,18,8,1152]{3,2,0,1:T(8,128)(2,1)S(1)} copy(bf16[2,18,8,1152]{1,0,3,2:T(2,128)(2,1)} %bitcast.37) | data formatting | bytes 1327104 | tf_op jit(solution)/shard_map/all_to_all | solution.py:72
  93.3 1.0 fusion.11
  94.3 1.0 fusion.1
  95.4 0.4 convert_element_type.72
  95.8 15.1 %all_to_all.36 = bf16[144,4,288]{2,1,0:T(4,128)(2,1)S(1)} all-to-all(bf16[144,4,288]{2,1,0:T(4,128)(2,1)S(1)} %convert_element_type.72), channel_id=1, replica_groups=mesh['row'=4,'col'=8] {'row'}, dimensions={0} | all-to-all | bytes 663552 | tf_op jit(solution)/shard_map/all_to_all | solution.py:116
  111.3 3.3 %convolution_convert_fusion = bf16[144,2048]{1,0:T(8,128)(2,1)S(1)} fusion(bf16[144,1152]{1,0:T(8,128)(2,1)S(1)} %reshape.199, bf16[1152,2048]{1,0:T(8,128)(2,1)} %param.7), kind=kOutput, calls=%fused_computation.6 | convolution fusion | flops 679772160 | bytes 5640192 | tf_op jit(solution)/shard_map/dot_general | solution.py:117
  114.6 1.0 reshape.200
  (20 shorter events, 2.4 us)
Async XLA Ops:
  12.7 24.0 %all-to-all-start = ((bf16[2,32,5184]{2,0,1:T(2,128)(2,1)}), bf16[2,32,5184]{2,0,1:T(2,128)(2,1)S(1)}, u32[]{:S(2)}, u32[]{:S(2)}) async-start(bf16[2,32,5184]{2,0,1:T(2,128)(2,1)} %copy.65), calls=%async_computation | async-start | bytes 1343488 | tf_op jit(solution)/shard_map/all_to_all | solution.py:111
where the time goes:
time: 116 us
  local copies, waits for them, and re-layouts  45.2 us (39%)
  blocking collectives  29.8 us (26%)
  waiting for transfers between devices  17.5 us (15%)
  matrix products  12.4 us (11%)
  starting transfers between devices  6.35 us (5%)
  other arithmetic  4.13 us (4%)
    unnamed x2, local copies, waits for them, and re-layouts  21.3 us
    all_to_all x1, waiting for transfers between devices, shards(): lax.all_to_all(stacked.astype(jnp.bfloat16), 'row', split_axis=1, concat_...  17.5 us
    all_to_all x1, blocking collectives, shards(): lax.all_to_all(spectrum, 'row', split_axis=0, concat_axis=2, tiled=True)  15.1 us
    all_to_all x1, blocking collectives, middle(): lax.all_to_all(turned.astype(jnp.bfloat16), 'col', split_axis=2, concat_a...  14.7 us
    convert_element_type x1, local copies, waits for them, and re-layouts, middle(): turned.astype(jnp.bfloat16)  7.94 us
    all_to_all x1, local copies, waits for them, and re-layouts, middle(): lax.all_to_all(turned.astype(jnp.bfloat16), 'col', split_axis=2, concat_a...  7.14 us
    all_to_all x1, starting transfers between devices, shards(): lax.all_to_all(stacked.astype(jnp.bfloat16), 'row', split_axis=1, concat_...  6.35 us
    dot_general x6, matrix products, product(): return jnp.dot(table, values, precision=highest)  4.34 us
  transfers between devices with their start and end apart: 1, of which 1 were waited for; matrix products, arithmetic and copies ran while one was open for 0% of the time, Pallas kernels for 0%

commit v1 on v0

--- a/solution.py
+++ b/solution.py
@@ -1,15 +1,293 @@
+import functools
 import math
 
 import jax
 import jax.numpy as jnp
+import numpy as np
 from jax import lax
+from jax.experimental import pallas as pl
+from jax.experimental.pallas import tpu as pltpu
 from jax.sharding import PartitionSpec as P
 
 GROUP = 128
+LANES = 128
+MESH = pl.DeviceIdType.MESH
 
 
 norm_eps = 1e-06
 highest = lax.Precision.HIGHEST
+
+
+def folded_list(length_first, devices):
+    block = length_first // devices
+    half = block // 2
+    result = np.zeros(length_first, np.int64)
+    for device in range(devices):
+        for inner in range(block):
+            if inner < half:
+                value = device * half + inner
+            elif device == 0 and inner == half:
+                value = length_first // 2
+            else:
+                value = length_first - device * half - (inner - half)
+            result[device * block + inner] = value % length_first
+    return result
+
+
+def channel_tables(row_count):
+    width = GROUP // row_count
+    half = width // 2
+    per_tile = LANES // width
+    j = np.arange(GROUP)
+    forward = np.zeros((row_count, per_tile * GROUP, LANES))
+    back = np.zeros((row_count, LANES, per_tile * GROUP))
+    for row in range(row_count):
+        for x in range(width):
+            m = row * half + x % half
+            cosine = x < half
+            column = np.cos(2 * np.pi * j * m / GROUP) if cosine else np.sin(2 * np.pi * j * m / GROUP)
+            entries = [(m, 1.0)]
+            if not cosine and m == 0:
+                column = np.cos(np.pi * j)
+                entries = [(GROUP // 2, 1.0)]
+            elif m:
+                entries = [(m, 1.0 if cosine else -1.0), (GROUP - m, 1.0)]
+            for g in range(per_tile):
+                forward[row, g * GROUP : (g + 1) * GROUP, g * width + x] = column
+                for at, sign in entries:
+                    back[row, g * width + x, g * GROUP + at] = sign
+    return forward, back
+
+
+def position_tables(rows_first, rows_second, row_count, col_count, padded):
+    length_first = rows_first * row_count
+    length_second = rows_second * col_count
+    positions = length_first * length_second
+    block = length_first // col_count
+    half = block // 2
+    a = np.arange(length_first)
+    first = np.zeros((col_count, col_count, padded, length_first, rows_second))
+    for col in range(col_count):
+        for i in range(rows_second):
+            p = a * length_second + col * rows_second + i
+            for target in range(col_count):
+                for f_at in range(half):
+                    f = target * half + f_at
+                    re_at, im_at = (2 * f_at) * rows_second + i, (2 * f_at + 1) * rows_second + i
+                    if f == 0:
+                        first[col, target, re_at, :, i] = 1.0
+                        first[col, target, im_at, :, i] = (-1.0) ** a
+                    else:
+                        angle = 2 * np.pi * (f * p % positions) / positions
+                        first[col, target, re_at, :, i] = np.cos(angle)
+                        first[col, target, im_at, :, i] = -np.sin(angle)
+    first = first.reshape(col_count, col_count * padded, length_first * rows_second)
+    k_b = np.arange(length_second)
+    second = np.zeros((2, 2, length_second, block, col_count, padded))
+    for other in range(2):
+        for s in range(block):
+            for source in range(col_count):
+                for i in range(rows_second):
+                    b = source * rows_second + i
+                    f_at, upper = s % half, s >= half
+                    re_at, im_at = (2 * f_at) * rows_second + i, (2 * f_at + 1) * rows_second + i
+                    if other == 0 and f_at == 0:
+                        shift = length_first // 2 if upper else 0
+                        angle = 2 * np.pi * (b * (k_b * length_first + shift) % positions) / positions
+                        at = im_at if upper else re_at
+                        second[other, 0, :, s, source, at] = np.cos(angle)
+                        second[other, 1, :, s, source, at] = np.sin(angle)
+                        continue
+                    sign = -1.0 if upper else 1.0
+                    angle = 2 * np.pi * (b * (k_b + (1 if upper else 0)) % length_second) / length_second
+                    second[other, 0, :, s, source, re_at] = np.cos(angle)
+                    second[other, 0, :, s, source, im_at] = np.sin(angle) * sign
+                    second[other, 1, :, s, source, re_at] = np.sin(angle)
+                    second[other, 1, :, s, source, im_at] = -np.cos(angle) * sign
+    second = second.reshape(2, 2, length_second * block, col_count * padded)
+    return first, second / math.sqrt(positions * GROUP)
+
+
+def kernel(
+    n_r, n_c, tokens, gain, w_in, w_out, forward, first, second, back, out,
+    tok_v, rows_v, norm_v, win_v, wout_v, forward_v, first_v, second_v, back_v,
+    sent1, came1, sent2, came2, sent3, came3, spec_v,
+    load_sem, self_sem, send_sem1, recv_sem1, send_sem2, recv_sem2, send_sem3, recv_sem3,
+):
+    row, col = lax.axis_index("row"), lax.axis_index("col")
+    rows_first, rows_second, features = tokens.shape
+    channels = w_in.shape[1]
+    tiles = sent1.shape[0]
+    span = n_r * GROUP
+
+    barrier = pltpu.get_barrier_semaphore()
+    for d in range(1, n_r):
+        pl.semaphore_signal(barrier, inc=1, device_id={"row": lax.rem(row + d, n_r)}, device_id_type=MESH)
+    for d in range(1, n_c):
+        pl.semaphore_signal(barrier, inc=1, device_id={"col": lax.rem(col + d, n_c)}, device_id_type=MESH)
+
+    spans = [(t * span, min(channels, (t + 1) * span)) for t in range(tiles)]
+    load_tok = pltpu.make_async_copy(tokens, tok_v, load_sem.at[0])
+    load_tok.start()
+    load_win = []
+    for t, (lo, hi) in enumerate(spans):
+        load_win.append(
+            pltpu.make_async_copy(w_in.at[:, lo:hi], win_v.at[:, lo:hi], load_sem.at[6 + t])
+        )
+    load_forward = pltpu.make_async_copy(forward, forward_v, load_sem.at[1])
+    load_first = pltpu.make_async_copy(first.at[col], first_v, load_sem.at[2])
+    load_second = pltpu.make_async_copy(second.at[jnp.minimum(col, 1)], second_v, load_sem.at[3])
+    load_back = pltpu.make_async_copy(back, back_v, load_sem.at[4])
+    load_wout = pltpu.make_async_copy(w_out, wout_v, load_sem.at[5])
+    load_win[0].start()
+    load_forward.start()
+    for copy in load_win[1:]:
+        copy.start()
+    load_first.start()
+    load_second.start()
+
+    load_tok.wait()
+    for a in range(rows_first):
+        rows_v[a * rows_second : (a + 1) * rows_second, :] = tok_v[a].astype(jnp.float32)
+    floats = rows_v[...]
+    inverse = lax.rsqrt(jnp.mean(floats * floats, axis=-1, keepdims=True) + norm_eps)
+    norm_v[...] = (floats * inverse * gain[...].astype(jnp.float32)).astype(jnp.bfloat16)
+
+    def exchange(sent, came, send_sem, recv_sem, self_sem_at, t, me, count, axis):
+        own = pltpu.make_async_copy(sent.at[t, me], came.at[t, me], self_sem_at)
+        own.start()
+        copies = [own]
+        for d in range(1, count):
+            target = lax.rem(me + d, count)
+            copy = pltpu.make_async_remote_copy(
+                src_ref=sent.at[t, target],
+                dst_ref=came.at[t, me],
+                send_sem=send_sem.at[t, d],
+                recv_sem=recv_sem.at[t, d],
+                device_id={axis: target},
+                device_id_type=MESH,
+            )
+            copy.start()
+            copies.append(copy)
+        return copies
+
+    steps1, steps2, steps3 = [], [], []
+    for t, (lo, hi) in enumerate(spans):
+        load_win[t].wait()
+        if t == 0:
+            load_forward.wait()
+        mapped = jnp.dot(norm_v[...], win_v[:, lo:hi], preferred_element_type=jnp.float32).astype(jnp.bfloat16)
+        for r in range(n_r):
+            piece = jnp.dot(mapped, forward_v[r, : hi - lo, :], preferred_element_type=jnp.float32)
+            sent1[t, r] = piece.astype(jnp.bfloat16)
+        if t == 0:
+            pl.semaphore_wait(barrier, n_r + n_c - 2)
+        steps1.append(exchange(sent1, came1, send_sem1, recv_sem1, self_sem.at[0, t], t, row, n_r, "row"))
+
+    load_back.start()
+    load_wout.start()
+    load_first.wait()
+    for t in range(tiles):
+        for copy in steps1[t]:
+            copy.wait()
+        values = came1[t].reshape(-1, LANES)
+        turned = jnp.dot(first_v[...], values, preferred_element_type=jnp.float32)
+        sent2[t] = turned.astype(jnp.bfloat16).reshape(sent2.shape[1:])
+        steps2.append(exchange(sent2, came2, send_sem2, recv_sem2, self_sem.at[1, t], t, col, n_c, "col"))
+
+    width = GROUP // n_r
+    lane = lax.broadcasted_iota(jnp.int32, (1, LANES), 1) % width
+    cosine = (lane < width // 2) | ((lane == width // 2) & (row == 0))
+    load_second.wait()
+    for t in range(tiles):
+        for copy in steps2[t]:
+            copy.wait()
+        values = came2[t].reshape(-1, LANES)
+        even = jnp.dot(second_v[0], values, preferred_element_type=jnp.float32)
+        odd = jnp.dot(second_v[1], values, preferred_element_type=jnp.float32)
+        both = jnp.where(cosine, even, odd)
+        sent3[t] = both.astype(jnp.bfloat16).reshape(sent3.shape[1:])
+        steps3.append(exchange(sent3, came3, send_sem3, recv_sem3, self_sem.at[2, t], t, row, n_r, "row"))
+
+    load_back.wait()
+    for t, (lo, hi) in enumerate(spans):
+        for copy in steps3[t]:
+            copy.wait()
+        total = jnp.dot(came3[t, 0], back_v[0, :, : hi - lo], preferred_element_type=jnp.float32)
+        for r in range(1, n_r):
+            total = total + jnp.dot(came3[t, r], back_v[r, :, : hi - lo], preferred_element_type=jnp.float32)
+        spec_v[:, lo:hi] = total.astype(jnp.bfloat16)
+    load_wout.wait()
+    out[...] = jnp.dot(spec_v[...], wout_v[...], preferred_element_type=jnp.float32).astype(jnp.bfloat16)
+
+
+def fused_shards(n_r, n_c, tokens, norm_gain, w_in, w_out):
+    rows_first, rows_second, features = tokens.shape
+    channels = w_in.shape[1]
+    length_first = rows_first * n_r
+    block = length_first // n_c
+    padded = -(-block * rows_second // 16) * 16
+    groups = channels // GROUP
+    tiles = -(-groups // n_r)
+    rows = rows_first * rows_second
+    length_second = rows_second * n_c
+    out_rows = length_second // n_r * block
+    forward, back = channel_tables(n_r)
+    first, second = position_tables(rows_first, rows_second, n_r, n_c, padded)
+    kind = jnp.bfloat16
+    tables = [jnp.asarray(np.asarray(x, np.float32).astype(kind)) for x in (forward, first, second, back)]
+    anywhere = pl.BlockSpec(memory_space=pl.ANY)
+    vmem = pl.BlockSpec(memory_space=pltpu.VMEM)
+    dma = pltpu.SemaphoreType.DMA
+    out = pl.pallas_call(
+        functools.partial(kernel, n_r, n_c),
+        out_shape=jax.ShapeDtypeStruct((out_rows, features), kind),
+        in_specs=[anywhere, vmem] + [anywhere] * 6,
+        out_specs=vmem,
+        scratch_shapes=[
+            pltpu.VMEM(tokens.shape, kind),
+            pltpu.VMEM((rows, features), jnp.float32),
+            pltpu.VMEM((rows, features), kind),
+            pltpu.VMEM(w_in.shape, kind),
+            pltpu.VMEM(w_out.shape, kind),
+            pltpu.VMEM(forward.shape, kind),
+            pltpu.VMEM(first.shape[1:], kind),
+            pltpu.VMEM(second.shape[1:], kind),
+            pltpu.VMEM(back.shape, kind),
+            pltpu.VMEM((tiles, n_r, rows, LANES), kind),
+            pltpu.VMEM((tiles, n_r, rows, LANES), kind),
+            pltpu.VMEM((tiles, n_c, padded, LANES), kind),
+            pltpu.VMEM((tiles, n_c, padded, LANES), kind),
+            pltpu.VMEM((tiles, n_r, out_rows, LANES), kind),
+            pltpu.VMEM((tiles, n_r, out_rows, LANES), kind),
+            pltpu.VMEM((out_rows, channels), kind),
+            dma((6 + tiles,)),
+            dma((3, tiles)),
+            dma((tiles, n_r)),
+            dma((tiles, n_r)),
+            dma((tiles, n_c)),
+            dma((tiles, n_c)),
+            dma((tiles, n_r)),
+            dma((tiles, n_r)),
+        ],
+        compiler_params=pltpu.CompilerParams(
+            collective_id=0, has_side_effects=True, vmem_limit_bytes=60 * 1024 * 1024
+        ),
+    )(tokens, norm_gain.reshape(1, -1), w_in, w_out, *tables)
+    return out.reshape(length_second // n_r, block, features)
+
+
+def fits(n_r, n_c, tokens_shape, channels):
+    length_first, length_second, _ = tokens_shape
+    rows = length_first // n_r * (length_second // n_c)
+    out_rows = length_second // n_r * (length_first // n_c)
+    return (
+        GROUP % (2 * n_r) == 0
+        and length_first % (2 * n_c) == 0
+        and rows % 16 == 0
+        and out_rows % 16 == 0
+        and length_second % n_r == 0
+    )
 
 
 def tables(length):
@@ -121,4 +399,13 @@
 def solution(mesh):
     in_specs = (P("row", "col", None), P(), P(), P())
     out_specs = P("row", "col", None)
-    return jax.shard_map(shards, mesh=mesh, in_specs=in_specs, out_specs=out_specs, check_vma=False)
+    n_r, n_c = mesh.shape["row"], mesh.shape["col"]
+
+    def run(tokens, norm_gain, w_in, w_out):
+        whole = fits(n_r, n_c, tokens.shape, w_in.shape[1])
+        body = functools.partial(fused_shards, n_r, n_c) if whole else shards
+        return jax.shard_map(body, mesh=mesh, in_specs=in_specs, out_specs=out_specs, check_vma=False)(
+            tokens, norm_gain, w_in, w_out
+        )
+
+    return run

time: 116 us -> 38.3 us (0.33)
  local copies, waits for them, and re-layouts: 45.2 us -> 5.83 us
  Pallas kernels: 0 us -> 32.3 us
  blocking collectives: 29.8 us -> 0 us
  waiting for transfers between devices: 17.5 us -> 0 us
  matrix products: 12.4 us -> 0 us
  starting transfers between devices: 6.35 us -> 0 us
  other arithmetic: 4.13 us -> 0 us
    pallas_call x0 -> x1, Pallas kernels: none -> 32.3 us  [fused_shards(): pl.pallas_call(functools.partial(kernel, n_r, n_c), out_shape=jax.ShapeDt...]
    all_to_all x2 -> x0, blocking collectives: 29.8 us -> none  [the longest x1 15.1 us: shards(): lax.all_to_all(spectrum, 'row', split_axis=0, concat_axis=2, tiled=True)]
    unnamed x2 -> x1, local copies, waits for them, and re-layouts: 21.3 us -> 2.29 us
    all_to_all x1 -> x0, waiting for transfers between devices: 17.5 us -> none  [shards(): lax.all_to_all(stacked.astype(jnp.bfloat16), 'row', split_axis=1, concat_...]
    dot_general x10 -> x0, matrix products: 12.4 us -> none  [the longest x6 4.34 us: product(): return jnp.dot(table, values, precision=highest)]
    convert_element_type x3 -> x0, local copies, waits for them, and re-layouts: 8.69 us -> none  [the longest x1 7.94 us: middle(): turned.astype(jnp.bfloat16)]
    all_to_all x2 -> x0, local copies, waits for them, and re-layouts: 7.31 us -> none  [the longest x1 7.14 us: middle(): lax.all_to_all(turned.astype(jnp.bfloat16), 'col', split_axis=2, concat_a...]
    all_to_all x1 -> x0, starting transfers between devices: 6.35 us -> none  [shards(): lax.all_to_all(stacked.astype(jnp.bfloat16), 'row', split_axis=1, concat_...]
  transfers between devices with their start and end apart: 1 -> 0, of which waited for: 1 -> 0; matrix products, arithmetic and copies ran while one was open for 0% -> 0% of each run, Pallas kernels for 0% -> 0%
where the time goes in v1:
time: 38.3 us; the launch traced here: 38.1 us
  Pallas kernels  32.3 us (84%)
  local copies, waits for them, and re-layouts  5.83 us (15%)
    pallas_call x1, Pallas kernels, fused_shards(): pl.pallas_call(functools.partial(kernel, n_r, n_c), out_shape=jax.ShapeDt...  32.3 us
    unnamed x1, local copies, waits for them, and re-layouts  2.29 us
    reshape x1, local copies, waits for them, and re-layouts, fused_shards(): return out.reshape(length_second // n_r, block, features)  2.25 us
    reshape x1, local copies, waits for them, and re-layouts, fused_shards(): norm_gain.reshape(1, -1)  1.29 us

profile of v1, /device:TPU:0, one launch (start us, length us, event | category | flops | bytes accessed | tf_op | source)
XLA Modules:
  0.0 38.1 jit_solution(11014252867811498082)
XLA Ops:
  0.0 1.3 %reshape.6.gain = bf16[1,2048]{1,0:T(2,128)(2,1)} reshape(bf16[2048]{0:T(1024)(128)(2,1)} %param.9) | data formatting | bytes 8192 | tf_op jit(solution)/shard_map/reshape | solution.py:276
  1.3 2.3 %copy.9.tokens = bf16[8,18,2048]{2,1,0:T(8,128)(2,1)} copy(bf16[8,18,2048]{2,0,1:T(8,128)(2,1)} %param.8) | data formatting | bytes 1179648 | tf_op args[0]
  3.6 32.3 %shard_map.82 = bf16[144,2048]{1,0:T(8,128)(2,1)} custom-call(bf16[8,18,2048]{2,1,0:T(8,128)(2,1)} %copy.9.tokens, bf16[1,2048]{1,0:T(2,128)(2,1)} %reshape.6.gain, bf16[2048,1152]{1,0:T(8,128)(2,1)} %w_in.1, bf16[1152,2048]{1,0:T(8,128)(2,1)} %w_out.1, bf16[4,512,128]{2,1,0:T(8,128)(2,1)} %constant.8.clone.forward, ...), custom_call_target="tpu_custom_call" | custom-call | tf_op jit(solution)/shard_map/pallas_call | solution.py:242
  35.8 2.2 %reshape.7 = bf16[36,4,2048]{2,1,0:T(4,128)(2,1)} reshape(bf16[144,2048]{1,0:T(8,128)(2,1)} %shard_map.82) | data formatting | bytes 1179648 | tf_op jit(solution)/shard_map/reshape | solution.py:277

commit v2 on v1

--- a/solution.py
+++ b/solution.py
@@ -11,6 +11,7 @@
 
 GROUP = 128
 LANES = 128
+SUBLANES = 16
 MESH = pl.DeviceIdType.MESH
 
 
@@ -59,66 +60,94 @@
     return forward, back
 
 
-def position_tables(rows_first, rows_second, row_count, col_count, padded):
+def position_tables(rows_first, rows_second, row_count, col_count, chunk, chunks):
     length_first = rows_first * row_count
     length_second = rows_second * col_count
     positions = length_first * length_second
     block = length_first // col_count
     half = block // 2
     a = np.arange(length_first)
-    first = np.zeros((col_count, col_count, padded, length_first, rows_second))
+    first = np.zeros((col_count, chunks, col_count, block, chunk, row_count, chunk, rows_first))
     for col in range(col_count):
         for i in range(rows_second):
+            at, j = divmod(i, chunk)
             p = a * length_second + col * rows_second + i
             for target in range(col_count):
                 for f_at in range(half):
                     f = target * half + f_at
-                    re_at, im_at = (2 * f_at) * rows_second + i, (2 * f_at + 1) * rows_second + i
+                    angle = 2 * np.pi * (f * p % positions) / positions
+                    real, imag = np.cos(angle), -np.sin(angle)
                     if f == 0:
-                        first[col, target, re_at, :, i] = 1.0
-                        first[col, target, im_at, :, i] = (-1.0) ** a
-                    else:
-                        angle = 2 * np.pi * (f * p % positions) / positions
-                        first[col, target, re_at, :, i] = np.cos(angle)
-                        first[col, target, im_at, :, i] = -np.sin(angle)
-    first = first.reshape(col_count, col_count * padded, length_first * rows_second)
+                        real, imag = np.ones(length_first), (-1.0) ** a
+                    first[col, at, target, 2 * f_at, j, :, j, :] = real.reshape(row_count, rows_first)
+                    first[col, at, target, 2 * f_at + 1, j, :, j, :] = imag.reshape(row_count, rows_first)
+    first = first.reshape(col_count, chunks, col_count * block * chunk, row_count, chunk * rows_first)
+    rest = rows_second - (chunks - 1) * chunk
+    last = first[:, -1, :, :, : rest * rows_first].reshape(col_count, col_count * block * chunk, -1)
+    first = first.reshape(col_count, chunks, col_count * block * chunk, -1)
+    first[:, -1] = 0.0
+    first[:, -1, :, : last.shape[-1]] = last
     k_b = np.arange(length_second)
-    second = np.zeros((2, 2, length_second, block, col_count, padded))
+    second = np.zeros((2, 2, length_second, block, col_count, chunks, block, chunk))
     for other in range(2):
         for s in range(block):
             for source in range(col_count):
                 for i in range(rows_second):
                     b = source * rows_second + i
                     f_at, upper = s % half, s >= half
-                    re_at, im_at = (2 * f_at) * rows_second + i, (2 * f_at + 1) * rows_second + i
+                    at, j = divmod(i, chunk)
+                    re_at, im_at = (source, at, 2 * f_at, j), (source, at, 2 * f_at + 1, j)
                     if other == 0 and f_at == 0:
                         shift = length_first // 2 if upper else 0
                         angle = 2 * np.pi * (b * (k_b * length_first + shift) % positions) / positions
-                        at = im_at if upper else re_at
-                        second[other, 0, :, s, source, at] = np.cos(angle)
-                        second[other, 1, :, s, source, at] = np.sin(angle)
+                        place = im_at if upper else re_at
+                        second[(other, 0, slice(None), s) + place] = np.cos(angle)
+                        second[(other, 1, slice(None), s) + place] = np.sin(angle)
                         continue
                     sign = -1.0 if upper else 1.0
                     angle = 2 * np.pi * (b * (k_b + (1 if upper else 0)) % length_second) / length_second
-                    second[other, 0, :, s, source, re_at] = np.cos(angle)
-                    second[other, 0, :, s, source, im_at] = np.sin(angle) * sign
-                    second[other, 1, :, s, source, re_at] = np.sin(angle)
-                    second[other, 1, :, s, source, im_at] = -np.cos(angle) * sign
-    second = second.reshape(2, 2, length_second * block, col_count * padded)
+                    second[(other, 0, slice(None), s) + re_at] = np.cos(angle)
+                    second[(other, 0, slice(None), s) + im_at] = np.sin(angle) * sign
+                    second[(other, 1, slice(None), s) + re_at] = np.sin(angle)
+                    second[(other, 1, slice(None), s) + im_at] = -np.cos(angle) * sign
+    second = second.reshape(2, 2, length_second * block, col_count * chunks * block * chunk)
     return first, second / math.sqrt(positions * GROUP)
 
 
+def widened(packed, parts, used):
+    count, rows, lanes = packed.shape
+    flat = packed.reshape(count * rows, lanes).astype(jnp.float32)
+    keep = lax.broadcasted_iota(jnp.int32, (1, lanes), 1) < used
+    blocks = []
+    for p in range(parts):
+        block = flat if p == 0 else pltpu.roll(flat, lanes - p * used, 1)
+        blocks.append(jnp.where(keep, block, 0.0).astype(packed.dtype).reshape(count, rows, lanes))
+    return blocks
+
+
+def packed_rows(values, parts, used):
+    rows = values.shape[0] // parts
+    total = values[:rows]
+    for p in range(1, parts):
+        total = total + pltpu.roll(values[p * rows : (p + 1) * rows], p * used, 1)
+    return total
+
+
 def kernel(
-    n_r, n_c, tokens, gain, w_in, w_out, forward, first, second, back, out,
-    tok_v, rows_v, norm_v, win_v, wout_v, forward_v, first_v, second_v, back_v,
-    sent1, came1, sent2, came2, sent3, came3, spec_v,
+    n_r, n_c, parts, tokens, gain, w_in, w_out, forward, first, second, back, out,
+    tok_v, norm_v, win_v, wout_v, forward_v, first_v, second_v, back_v,
+    sent1, came1, sent2, came2, sent3, came3, wide_v, wide3_v, acc_v,
     load_sem, self_sem, send_sem1, recv_sem1, send_sem2, recv_sem2, send_sem3, recv_sem3,
 ):
     row, col = lax.axis_index("row"), lax.axis_index("col")
-    rows_first, rows_second, features = tokens.shape
+    rows, features = tokens.shape
     channels = w_in.shape[1]
     tiles = sent1.shape[0]
     span = n_r * GROUP
+    spans = [(t * span, min(channels, (t + 1) * span)) for t in range(tiles)]
+    width = GROUP // n_r
+    used = (spans[-1][1] - spans[-1][0]) // GROUP * width
+    order = [tiles - 1] + list(range(tiles - 1))
 
     barrier = pltpu.get_barrier_semaphore()
     for d in range(1, n_r):
@@ -126,42 +155,44 @@
     for d in range(1, n_c):
         pl.semaphore_signal(barrier, inc=1, device_id={"col": lax.rem(col + d, n_c)}, device_id_type=MESH)
 
-    spans = [(t * span, min(channels, (t + 1) * span)) for t in range(tiles)]
     load_tok = pltpu.make_async_copy(tokens, tok_v, load_sem.at[0])
     load_tok.start()
-    load_win = []
-    for t, (lo, hi) in enumerate(spans):
-        load_win.append(
-            pltpu.make_async_copy(w_in.at[:, lo:hi], win_v.at[:, lo:hi], load_sem.at[6 + t])
-        )
+    load_win = [
+        pltpu.make_async_copy(w_in.at[:, lo:hi], win_v.at[:, lo:hi], load_sem.at[6 + t])
+        for t, (lo, hi) in enumerate(spans)
+    ]
     load_forward = pltpu.make_async_copy(forward, forward_v, load_sem.at[1])
     load_first = pltpu.make_async_copy(first.at[col], first_v, load_sem.at[2])
     load_second = pltpu.make_async_copy(second.at[jnp.minimum(col, 1)], second_v, load_sem.at[3])
     load_back = pltpu.make_async_copy(back, back_v, load_sem.at[4])
     load_wout = pltpu.make_async_copy(w_out, wout_v, load_sem.at[5])
-    load_win[0].start()
+    load_win[order[0]].start()
     load_forward.start()
-    for copy in load_win[1:]:
-        copy.start()
+    for t in order[1:]:
+        load_win[t].start()
     load_first.start()
     load_second.start()
 
     load_tok.wait()
-    for a in range(rows_first):
-        rows_v[a * rows_second : (a + 1) * rows_second, :] = tok_v[a].astype(jnp.float32)
-    floats = rows_v[...]
+    floats = tok_v[...].astype(jnp.float32)
     inverse = lax.rsqrt(jnp.mean(floats * floats, axis=-1, keepdims=True) + norm_eps)
-    norm_v[...] = (floats * inverse * gain[...].astype(jnp.float32)).astype(jnp.bfloat16)
+    gains = gain[...].astype(jnp.float32)
+    for at in range(features // LANES):
+        lanes = slice(at * LANES, (at + 1) * LANES)
+        scaled = tok_v[:, lanes].astype(jnp.float32) * inverse * gains[at : at + 1, :]
+        norm_v[:, lanes] = scaled.astype(jnp.bfloat16)
 
     def exchange(sent, came, send_sem, recv_sem, self_sem_at, t, me, count, axis):
-        own = pltpu.make_async_copy(sent.at[t, me], came.at[t, me], self_sem_at)
-        own.start()
-        copies = [own]
-        for d in range(1, count):
+        size = sent.shape[2]
+        if axis == "row" and t == tiles - 1:
+            size = size // parts
+        own = pltpu.make_async_copy(sent.at[t, me, 0:size], came.at[t, me, 0:size], self_sem_at)
+        copies = []
+        for d in sorted(range(1, count), key=lambda d: -min(d, count - d)):
             target = lax.rem(me + d, count)
             copy = pltpu.make_async_remote_copy(
-                src_ref=sent.at[t, target],
-                dst_ref=came.at[t, me],
+                src_ref=sent.at[t, target, 0:size],
+                dst_ref=came.at[t, me, 0:size],
                 send_sem=send_sem.at[t, d],
                 recv_sem=recv_sem.at[t, d],
                 device_id={axis: target},
@@ -169,56 +200,90 @@
             )
             copy.start()
             copies.append(copy)
-        return copies
-
-    steps1, steps2, steps3 = [], [], []
-    for t, (lo, hi) in enumerate(spans):
+        own.start()
+        return [own] + copies
+
+    steps1, steps2, steps3 = {}, {}, {}
+    for t in order:
+        lo, hi = spans[t]
         load_win[t].wait()
-        if t == 0:
+        mapped = jnp.dot(norm_v[...], win_v[:, lo:hi], preferred_element_type=jnp.float32).astype(jnp.bfloat16)
+        if t == order[0]:
             load_forward.wait()
-        mapped = jnp.dot(norm_v[...], win_v[:, lo:hi], preferred_element_type=jnp.float32).astype(jnp.bfloat16)
         for r in range(n_r):
             piece = jnp.dot(mapped, forward_v[r, : hi - lo, :], preferred_element_type=jnp.float32)
-            sent1[t, r] = piece.astype(jnp.bfloat16)
-        if t == 0:
+            if t == tiles - 1:
+                sent1[t, r, 0 : rows // parts] = packed_rows(piece, parts, used).astype(jnp.bfloat16)
+            else:
+                sent1[t, r] = piece.astype(jnp.bfloat16)
+        if t == order[0]:
             pl.semaphore_wait(barrier, n_r + n_c - 2)
-        steps1.append(exchange(sent1, came1, send_sem1, recv_sem1, self_sem.at[0, t], t, row, n_r, "row"))
+        steps1[t] = exchange(sent1, came1, send_sem1, recv_sem1, self_sem.at[0, t], t, row, n_r, "row")
 
     load_back.start()
     load_wout.start()
     load_first.wait()
-    for t in range(tiles):
+    chunks, high, depth = first_v.shape
+    step = depth // n_r
+    height = high // n_c
+    for t in order:
         for copy in steps1[t]:
             copy.wait()
-        values = came1[t].reshape(-1, LANES)
-        turned = jnp.dot(first_v[...], values, preferred_element_type=jnp.float32)
-        sent2[t] = turned.astype(jnp.bfloat16).reshape(sent2.shape[1:])
-        steps2.append(exchange(sent2, came2, send_sem2, recv_sem2, self_sem.at[1, t], t, col, n_c, "col"))
-
-    width = GROUP // n_r
+        source = came1.at[t]
+        if t == tiles - 1:
+            size = rows // parts
+            for p, block in enumerate(widened(came1[t, :, 0:size], parts, used)):
+                wide_v[:, p * size : (p + 1) * size] = block
+            source = wide_v
+        for at in range(chunks):
+            values = source[:, at * step : min(rows, (at + 1) * step)]
+            values = values.reshape(-1, LANES)
+            turned = jnp.dot(first_v[at, :, : values.shape[0]], values, preferred_element_type=jnp.float32)
+            turned = turned.astype(jnp.bfloat16).reshape(n_c, height, LANES)
+            sent2[t, :, at * height : (at + 1) * height] = turned
+        steps2[t] = exchange(sent2, came2, send_sem2, recv_sem2, self_sem.at[1, t], t, col, n_c, "col")
+
     lane = lax.broadcasted_iota(jnp.int32, (1, LANES), 1) % width
     cosine = (lane < width // 2) | ((lane == width // 2) & (row == 0))
     load_second.wait()
-    for t in range(tiles):
+    out_rows = sent3.shape[2]
+    for t in order:
         for copy in steps2[t]:
             copy.wait()
         values = came2[t].reshape(-1, LANES)
         even = jnp.dot(second_v[0], values, preferred_element_type=jnp.float32)
         odd = jnp.dot(second_v[1], values, preferred_element_type=jnp.float32)
         both = jnp.where(cosine, even, odd)
-        sent3[t] = both.astype(jnp.bfloat16).reshape(sent3.shape[1:])
-        steps3.append(exchange(sent3, came3, send_sem3, recv_sem3, self_sem.at[2, t], t, row, n_r, "row"))
+        if t == tiles - 1:
+            for r in range(n_r):
+                block = packed_rows(both[r * out_rows : (r + 1) * out_rows], parts, used)
+                sent3[t, r, 0 : out_rows // parts] = block.astype(jnp.bfloat16)
+        else:
+            sent3[t] = both.astype(jnp.bfloat16).reshape(sent3.shape[1:])
+        steps3[t] = exchange(sent3, came3, send_sem3, recv_sem3, self_sem.at[2, t], t, row, n_r, "row")
 
     load_back.wait()
-    for t, (lo, hi) in enumerate(spans):
+    load_wout.wait()
+    for t in order:
+        lo, hi = spans[t]
         for copy in steps3[t]:
             copy.wait()
-        total = jnp.dot(came3[t, 0], back_v[0, :, : hi - lo], preferred_element_type=jnp.float32)
+        source = came3.at[t]
+        if t == tiles - 1:
+            size = out_rows // parts
+            for p, block in enumerate(widened(came3[t, :, 0:size], parts, used)):
+                wide3_v[:, p * size : (p + 1) * size] = block
+            source = wide3_v
+        total = jnp.dot(source[0], back_v[0, :, : hi - lo], preferred_element_type=jnp.float32)
         for r in range(1, n_r):
-            total = total + jnp.dot(came3[t, r], back_v[r, :, : hi - lo], preferred_element_type=jnp.float32)
-        spec_v[:, lo:hi] = total.astype(jnp.bfloat16)
-    load_wout.wait()
-    out[...] = jnp.dot(spec_v[...], wout_v[...], preferred_element_type=jnp.float32).astype(jnp.bfloat16)
+            total = total + jnp.dot(source[r], back_v[r, :, : hi - lo], preferred_element_type=jnp.float32)
+        share = jnp.dot(total.astype(jnp.bfloat16), wout_v[lo:hi, :], preferred_element_type=jnp.float32)
+        if t == order[0]:
+            acc_v[...] = share
+        elif t != order[-1]:
+            acc_v[...] += share
+        else:
+            out[...] = (acc_v[...] + share).reshape(out.shape).astype(jnp.bfloat16)
 
 
 def fused_shards(n_r, n_c, tokens, norm_gain, w_in, w_out):
@@ -226,27 +291,31 @@
     channels = w_in.shape[1]
     length_first = rows_first * n_r
     block = length_first // n_c
-    padded = -(-block * rows_second // 16) * 16
+    chunk = SUBLANES // block
+    chunks = -(-rows_second // chunk)
+    padded = chunks * SUBLANES
     groups = channels // GROUP
     tiles = -(-groups // n_r)
     rows = rows_first * rows_second
     length_second = rows_second * n_c
     out_rows = length_second // n_r * block
     forward, back = channel_tables(n_r)
-    first, second = position_tables(rows_first, rows_second, n_r, n_c, padded)
+    first, second = position_tables(rows_first, rows_second, n_r, n_c, chunk, chunks)
+    used = (groups - (tiles - 1) * n_r) * (GROUP // n_r)
+    parts = max(p for p in range(1, LANES // used + 1) if rows % (SUBLANES * p) == 0 and out_rows % (SUBLANES * p) == 0)
+    tokens = tokens.transpose(1, 0, 2).reshape(rows, features)
     kind = jnp.bfloat16
     tables = [jnp.asarray(np.asarray(x, np.float32).astype(kind)) for x in (forward, first, second, back)]
     anywhere = pl.BlockSpec(memory_space=pl.ANY)
     vmem = pl.BlockSpec(memory_space=pltpu.VMEM)
     dma = pltpu.SemaphoreType.DMA
     out = pl.pallas_call(
-        functools.partial(kernel, n_r, n_c),
-        out_shape=jax.ShapeDtypeStruct((out_rows, features), kind),
+        functools.partial(kernel, n_r, n_c, parts),
+        out_shape=jax.ShapeDtypeStruct((length_second // n_r, block, features), kind),
         in_specs=[anywhere, vmem] + [anywhere] * 6,
         out_specs=vmem,
         scratch_shapes=[
             pltpu.VMEM(tokens.shape, kind),
-            pltpu.VMEM((rows, features), jnp.float32),
             pltpu.VMEM((rows, features), kind),
             pltpu.VMEM(w_in.shape, kind),
             pltpu.VMEM(w_out.shape, kind),
@@ -260,7 +329,9 @@
             pltpu.VMEM((tiles, n_c, padded, LANES), kind),
             pltpu.VMEM((tiles, n_r, out_rows, LANES), kind),
             pltpu.VMEM((tiles, n_r, out_rows, LANES), kind),
-            pltpu.VMEM((out_rows, channels), kind),
+            pltpu.VMEM((n_r, rows, LANES), kind),
+            pltpu.VMEM((n_r, out_rows, LANES), kind),
+            pltpu.VMEM((out_rows, features), jnp.float32),
             dma((6 + tiles,)),
             dma((3, tiles)),
             dma((tiles, n_r)),
@@ -273,8 +344,8 @@
         compiler_params=pltpu.CompilerParams(
             collective_id=0, has_side_effects=True, vmem_limit_bytes=60 * 1024 * 1024
         ),
-    )(tokens, norm_gain.reshape(1, -1), w_in, w_out, *tables)
-    return out.reshape(length_second // n_r, block, features)
+    )(tokens, norm_gain.reshape(-1, LANES), w_in, w_out, *tables)
+    return out
 
 
 def fits(n_r, n_c, tokens_shape, channels):
@@ -284,8 +355,10 @@
     return (
         GROUP % (2 * n_r) == 0
         and length_first % (2 * n_c) == 0
-        and rows % 16 == 0
-        and out_rows % 16 == 0
+        and SUBLANES % (length_first // n_c) == 0
+        and rows % SUBLANES == 0
+        and out_rows % SUBLANES == 0
+        and length_first // n_r * (SUBLANES // (length_first // n_c)) % SUBLANES == 0
         and length_second % n_r == 0
     )
 

time: 38.3 us -> 31.6 us (0.83)
  local copies, waits for them, and re-layouts: 5.83 us -> 2.15 us
  Pallas kernels: 32.3 us -> 29.3 us
    reshape x2 -> x0, local copies, waits for them, and re-layouts: 3.54 us -> none  [the longest x1 2.25 us: fused_shards(): return out.reshape(length_second // n_r, block, features)]
    pallas_call x1, Pallas kernels: 32.3 us -> 29.3 us  [fused_shards(): pl.pallas_call(functools.partial(kernel, n_r, n_c, parts), out_shape=jax....]
where the time goes in v2:
time: 31.6 us; the launch traced here: 31.4 us
  Pallas kernels  29.3 us (93%)
  local copies, waits for them, and re-layouts  2.15 us (7%)
    pallas_call x1, Pallas kernels, fused_shards(): pl.pallas_call(functools.partial(kernel, n_r, n_c, parts), out_shape=jax....  29.3 us
    unnamed x1, local copies, waits for them, and re-layouts  2.15 us

profile of v2, /device:TPU:0, one launch (start us, length us, event | category | flops | bytes accessed | tf_op | source)
XLA Modules:
  0.0 31.4 jit_solution(3456995021548587695)
XLA Ops:
  0.0 29.3 %shard_map.82 = bf16[36,4,2048]{2,1,0:T(4,128)(2,1)} custom-call(bf16[144,2048]{1,0:T(8,128)(2,1)} %bitcast.4, bf16[16,128]{1,0:T(8,128)(2,1)} %bitcast.5, bf16[2048,1152]{1,0:T(8,128)(2,1)} %w_in.1, bf16[1152,2048]{1,0:T(8,128)(2,1)} %w_out.1, bf16[4,512,128]{2,1,0:T(8,128)(2,1)} %constant.8.clone.forward, bf16[8,5,128,128]{3,2,1,0:T(8,128)(2,1)} %constant.9.clone.first, ...), custom_call_target="tpu_custom_call" | custom-call | tf_op jit(solution)/shard_map/pallas_call | solution.py:312
  29.3 2.1 %copy.10 = bf16[36,4,2048]{2,1,0:T(4,128)(2,1)} copy(bf16[36,4,2048]{2,1,0:T(4,128)(2,1)} %shard_map.82) | data formatting | bytes 1179648

commit v3 on v2

--- a/solution.py
+++ b/solution.py
@@ -134,9 +134,9 @@
 
 
 def kernel(
-    n_r, n_c, parts, tokens, gain, w_in, w_out, forward, first, second, back, out,
-    tok_v, norm_v, win_v, wout_v, forward_v, first_v, second_v, back_v,
-    sent1, came1, sent2, came2, sent3, came3, wide_v, wide3_v, acc_v,
+    n_r, n_c, parts, tokens, gain, w_in, forward, first, second, back, out,
+    tok_v, norm_v, win_v, forward_v, first_v, second_v, back_v,
+    sent1, came1, sent2, came2, sent3, came3, wide_v, wide3_v,
     load_sem, self_sem, send_sem1, recv_sem1, send_sem2, recv_sem2, send_sem3, recv_sem3,
 ):
     row, col = lax.axis_index("row"), lax.axis_index("col")
@@ -165,7 +165,6 @@
     load_first = pltpu.make_async_copy(first.at[col], first_v, load_sem.at[2])
     load_second = pltpu.make_async_copy(second.at[jnp.minimum(col, 1)], second_v, load_sem.at[3])
     load_back = pltpu.make_async_copy(back, back_v, load_sem.at[4])
-    load_wout = pltpu.make_async_copy(w_out, wout_v, load_sem.at[5])
     load_win[order[0]].start()
     load_forward.start()
     for t in order[1:]:
@@ -221,7 +220,6 @@
         steps1[t] = exchange(sent1, came1, send_sem1, recv_sem1, self_sem.at[0, t], t, row, n_r, "row")
 
     load_back.start()
-    load_wout.start()
     load_first.wait()
     chunks, high, depth = first_v.shape
     step = depth // n_r
@@ -263,7 +261,6 @@
         steps3[t] = exchange(sent3, came3, send_sem3, recv_sem3, self_sem.at[2, t], t, row, n_r, "row")
 
     load_back.wait()
-    load_wout.wait()
     for t in order:
         lo, hi = spans[t]
         for copy in steps3[t]:
@@ -277,13 +274,12 @@
         total = jnp.dot(source[0], back_v[0, :, : hi - lo], preferred_element_type=jnp.float32)
         for r in range(1, n_r):
             total = total + jnp.dot(source[r], back_v[r, :, : hi - lo], preferred_element_type=jnp.float32)
-        share = jnp.dot(total.astype(jnp.bfloat16), wout_v[lo:hi, :], preferred_element_type=jnp.float32)
-        if t == order[0]:
-            acc_v[...] = share
-        elif t != order[-1]:
-            acc_v[...] += share
-        else:
-            out[...] = (acc_v[...] + share).reshape(out.shape).astype(jnp.bfloat16)
+        out[:, lo:hi] = total.astype(jnp.bfloat16)
+
+
+def last_product(spectrum, w_out, out):
+    total = jnp.dot(spectrum[...], w_out[...], preferred_element_type=jnp.float32)
+    out[...] = total.reshape(out.shape).astype(jnp.bfloat16)
 
 
 def fused_shards(n_r, n_c, tokens, norm_gain, w_in, w_out):
@@ -309,16 +305,15 @@
     anywhere = pl.BlockSpec(memory_space=pl.ANY)
     vmem = pl.BlockSpec(memory_space=pltpu.VMEM)
     dma = pltpu.SemaphoreType.DMA
-    out = pl.pallas_call(
+    spectrum = pl.pallas_call(
         functools.partial(kernel, n_r, n_c, parts),
-        out_shape=jax.ShapeDtypeStruct((length_second // n_r, block, features), kind),
-        in_specs=[anywhere, vmem] + [anywhere] * 6,
+        out_shape=jax.ShapeDtypeStruct((out_rows, channels), kind),
+        in_specs=[anywhere, vmem] + [anywhere] * 5,
         out_specs=vmem,
         scratch_shapes=[
             pltpu.VMEM(tokens.shape, kind),
             pltpu.VMEM((rows, features), kind),
             pltpu.VMEM(w_in.shape, kind),
-            pltpu.VMEM(w_out.shape, kind),
             pltpu.VMEM(forward.shape, kind),
             pltpu.VMEM(first.shape[1:], kind),
             pltpu.VMEM(second.shape[1:], kind),
@@ -331,7 +326,6 @@
             pltpu.VMEM((tiles, n_r, out_rows, LANES), kind),
             pltpu.VMEM((n_r, rows, LANES), kind),
             pltpu.VMEM((n_r, out_rows, LANES), kind),
-            pltpu.VMEM((out_rows, features), jnp.float32),
             dma((6 + tiles,)),
             dma((3, tiles)),
             dma((tiles, n_r)),
@@ -342,10 +336,16 @@
             dma((tiles, n_r)),
         ],
         compiler_params=pltpu.CompilerParams(
-            collective_id=0, has_side_effects=True, vmem_limit_bytes=60 * 1024 * 1024
+            collective_id=0, has_side_effects=True, vmem_limit_bytes=53 * 1024 * 1024
         ),
-    )(tokens, norm_gain.reshape(-1, LANES), w_in, w_out, *tables)
-    return out
+    )(tokens, norm_gain.reshape(-1, LANES), w_in, *tables)
+    return pl.pallas_call(
+        last_product,
+        out_shape=jax.ShapeDtypeStruct((length_second // n_r, block, features), kind),
+        in_specs=[vmem] * 2,
+        out_specs=vmem,
+        compiler_params=pltpu.CompilerParams(vmem_limit_bytes=16 * 1024 * 1024),
+    )(spectrum, w_out)
 
 
 def fits(n_r, n_c, tokens_shape, channels):

time: 31.6 us -> 30.9 us (0.978)
  local copies, waits for them, and re-layouts: 2.15 us -> 1.73 us
  Pallas kernels: 29.3 us -> 28.9 us
    pallas_call x1, Pallas kernels: 29.3 us -> 27.1 us  [fused_shards(): pl.pallas_call(functools.partial(kernel, n_r, n_c, parts), out_shape=jax....]
    pallas_call x0 -> x1, Pallas kernels: none -> 1.86 us  [fused_shards(): pl.pallas_call(last_product, out_shape=jax.ShapeDtypeStruct((length_secon...]
    unnamed x1 -> x6, local copies, waits for them, and re-layouts: 2.15 us -> 1.73 us
where the time goes in v3:
time: 30.9 us; the launch traced here: 30.7 us
  Pallas kernels  28.9 us (94%)
  local copies, waits for them, and re-layouts  1.73 us (6%)
    pallas_call x1, Pallas kernels, fused_shards(): pl.pallas_call(functools.partial(kernel, n_r, n_c, parts), out_shape=jax....  27.1 us
    pallas_call x1, Pallas kernels, fused_shards(): pl.pallas_call(last_product, out_shape=jax.ShapeDtypeStruct((length_secon...  1.86 us
    unnamed x6, local copies, waits for them, and re-layouts  1.73 us

profile of v3, /device:TPU:0, one launch (start us, length us, event | category | flops | bytes accessed | tf_op | source)
XLA Modules:
  0.0 30.7 jit_solution(10925504428118059262)
XLA Ops:
  0.0 0.0 copy-start.1
  0.0 1.0 %copy-done.1 = bf16[4,512,128]{2,1,0:T(8,128)(2,1)S(1)} copy-done((bf16[4,512,128]{2,1,0:T(8,128)(2,1)S(1)}, bf16[4,512,128]{2,1,0:T(8,128)(2,1)}, u32[]{:S(2)}) %copy-start.1) | copy-done | bytes 524312
  1.0 0.0 copy-start.2
  1.0 0.7 %copy-done.2 = bf16[2048]{0:T(1024)(128)(2,1)S(1)} copy-done((bf16[2048]{0:T(1024)(128)(2,1)S(1)}, bf16[2048]{0:T(1024)(128)(2,1)}, u32[]{:S(2)}) %copy-start.2) | copy-done | bytes 4120
  1.7 0.0 copy-start
  1.7 27.1 %shard_map.82.spectrum = bf16[144,1152]{1,0:T(8,128)(2,1)S(1)} custom-call(bf16[144,2048]{1,0:T(8,128)(2,1)} %bitcast.5, bf16[16,128]{1,0:T(8,128)(2,1)S(1)} %bitcast.4, bf16[2048,1152]{1,0:T(8,128)(2,1)} %w_in.1, bf16[4,512,128]{2,1,0:T(8,128)(2,1)S(1)} %copy-done.1, bf16[8,5,128,128]{3,2,1,0:T(8,128)(2,1)} %constant.9.clone.first, ...), custom_call_target="tpu_custom_call" | custom-call | tf_op jit(solution)/shard_map/pallas_call | solution.py:308
  28.8 0.0 copy-done
  28.8 1.9 %shard_map.83 = bf16[36,4,2048]{2,1,0:T(4,128)(2,1)} custom-call(bf16[144,1152]{1,0:T(8,128)(2,1)S(1)} %shard_map.82.spectrum, bf16[1152,2048]{1,0:T(8,128)(2,1)S(1)} %copy-done), custom_call_target="tpu_custom_call" | custom-call | tf_op jit(solution)/shard_map/pallas_call | solution.py:342
Async XLA Ops:
  0.0 1.0 %copy-start.1 = (bf16[4,512,128]{2,1,0:T(8,128)(2,1)S(1)}, bf16[4,512,128]{2,1,0:T(8,128)(2,1)}, u32[]{:S(2)}) copy-start(bf16[4,512,128]{2,1,0:T(8,128)(2,1)} %constant.8.clone.forward) | copy-start | bytes 1572868
  1.0 0.7 %copy-start.2 = (bf16[2048]{0:T(1024)(128)(2,1)S(1)}, bf16[2048]{0:T(1024)(128)(2,1)}, u32[]{:S(2)}) copy-start(bf16[2048]{0:T(1024)(128)(2,1)} %param.9) | copy-start | bytes 12292
  1.7 27.1 %copy-start = (bf16[1152,2048]{1,0:T(8,128)(2,1)S(1)}, bf16[1152,2048]{1,0:T(8,128)(2,1)}, u32[]{:S(2)}) copy-start(bf16[1152,2048]{1,0:T(8,128)(2,1)} %w_out.1) | copy-start | bytes 14155780
